TPU v7x, 32 devices: a whole 2x2x4 slice. The times are simulated.
32 devices in a mesh: sp: 16 (over z, y, x), tp: 2 (over core).
Axes of the slice: x: 2, y: 2, z: 4, core: 2. Of those that a mesh axis runs over, the one named last changes fastest.
Arguments:
- hidden_in: bfloat16 [4096, 2048], P('sp', 'tp'), may hold values from -6 to 6
- w_query_rec: bfloat16 [2048, 2048], P('sp', 'tp'), may hold values from -0.125 to 0.125
- w_forget: bfloat16 [2048, 2048], P('sp', 'tp'), may hold values from -0.125 to 0.125
- w_input: bfloat16 [2048, 2048], P('sp', 'tp'), may hold values from -0.125 to 0.125
- forget_gap: float32 [2048], P('tp'), may hold values from 1e-05 to 0.08
- decay_extra: float32 [4096, 16], P('sp', 'tp'), may hold values from -0.75 to 0
- rec_gain: float32 [128], replicated, may hold values from 0.1 to 1.9
- w_q_down: bfloat16 [2048, 512], P(None, 'tp'), may hold values from -0.125 to 0.125
- w_kv_down: bfloat16 [2048, 256], P(None, 'tp'), may hold values from -0.125 to 0.125
- w_key_rope: bfloat16 [2048, 32], replicated, may hold values from -0.125 to 0.125
- q_gain: float32 [512], replicated, may hold values from 1.4 to 7
- kv_gain: float32 [256], replicated, may hold values from 1.4 to 7
- w_q_nope: bfloat16 [512, 1024], P(None, 'tp'), may hold values from -0.25 to 0.25
- w_q_rope: bfloat16 [512, 512], P(None, 'tp'), may hold values from -0.25 to 0.25
- w_k_up: bfloat16 [256, 1024], P(None, 'tp'), may hold values from -0.375 to 0.375
- w_v_up: bfloat16 [256, 1024], P(None, 'tp'), may hold values from -0.375 to 0.375
- w_out_rec: bfloat16 [2048, 2048], P('tp'), may hold values from -0.109375 to 0.109375
- w_out_att: bfloat16 [1024, 2048], P('tp'), may hold values from -0.109375 to 0.109375
Outputs:
- mixed_out: bfloat16 [4096, 2048], P(('sp', 'tp'))
All inputs are finite; a program needn't handle non-finite values.
Results may differ from a plain program's by a relative error of at most 0.02.
The roundings to bfloat16 on the way count: a program that leaves them out, or rounds other values in their place, can miss the bound.
Values may be sent and summed in bfloat16 or wider, within the bound.
A program may use at most 128 MiB of HBM per device.

v0:
```python
import math

import jax
import jax.numpy as jnp
from jax import lax
from jax.sharding import PartitionSpec as P

HG_KDIM = 128
HG_VDIM = 128
HG_BLOCK = 64
NOPE = 64
ROPE = 32
MLA_V = 64


NORM_EPS = 1e-06
ROPE_BASE = 10000.0
NEG_BIG = -1e30


def carried_in(part, axis, combine, identity):
    place = lax.axis_index(axis)
    gathered = jax.tree.map(lambda a: lax.all_gather(a, axis), part)
    state = jax.tree.map(lambda a, e: jnp.zeros_like(a) + jnp.asarray(e, a.dtype), part, identity)

    def one(step, state):
        return combine(
            state, jax.tree.map(lambda a: lax.dynamic_index_in_dim(a, step, 0, False), gathered)
        )

    return lax.fori_loop(0, place, one, state)


def rms_scale(values):
    return values * lax.rsqrt(jnp.mean(values * values, axis=-1, keepdims=True) + NORM_EPS)


def rotate_half(values, cosine, sine_table):
    half_width = values.shape[-1] // 2
    lower_half = values[..., :half_width]
    upper_half = values[..., half_width:]
    return jnp.concatenate(
        [
            lower_half * cosine - upper_half * sine_table,
            lower_half * sine_table + upper_half * cosine,
        ],
        axis=-1,
    )


def rotary_tables(row_count, offset, rot_width):
    positions = jnp.arange(row_count, dtype=jnp.float32) + offset
    frequency = 1.0 / ROPE_BASE ** (jnp.arange(0, rot_width, 2, dtype=jnp.float32) / rot_width)
    angles = positions[:, None] * frequency[None, :]
    return (jnp.cos(angles), jnp.sin(angles))


def block_step(rec_state, inputs):
    queries, key_in, values, log_forget = inputs
    cumulative = jnp.cumsum(log_forget, axis=1)
    log_gaps = cumulative[:, :, None, :] - cumulative[:, None, :, :]
    block_len = queries.shape[1]
    lower_mask = jnp.tril(jnp.ones((block_len, block_len), jnp.float32))
    decays = jnp.exp(jnp.minimum(log_gaps, 0.0)) * lower_mask[None, :, :, None]
    scores = jnp.einsum(
        "htsd,hsd->hts", queries[:, :, None, :] * decays, key_in, precision=lax.Precision.HIGHEST
    )
    block_out = jnp.einsum(
        "hts,hsv->htv", scores, values, precision=lax.Precision.HIGHEST
    ) + jnp.einsum(
        "htd,hdv->htv", queries * jnp.exp(cumulative), rec_state, precision=lax.Precision.HIGHEST
    )
    last_cumul = cumulative[:, -1:, :]
    rec_state = jnp.exp(last_cumul[:, 0, :])[..., None] * rec_state + jnp.einsum(
        "hsd,hsv->hdv",
        key_in * jnp.exp(last_cumul - cumulative),
        values,
        precision=lax.Precision.HIGHEST,
    )
    return (rec_state, block_out)


def score_block(q_nope, q_rope, k_nope, k_rope, values, q_start, k_start):
    score_scale = 1.0 / math.sqrt(NOPE + ROPE)
    scores = (
        jnp.einsum("qhd,khd->hqk", q_nope, k_nope, preferred_element_type=jnp.float32)
        + jnp.einsum("qhr,kr->hqk", q_rope, k_rope, preferred_element_type=jnp.float32)
    ) * score_scale
    q_pos = q_start + jnp.arange(q_nope.shape[0], dtype=jnp.int32)
    k_pos = k_start + jnp.arange(k_nope.shape[0], dtype=jnp.int32)
    allowed = k_pos[None, :] <= q_pos[:, None]
    scores = jnp.where(allowed[None], scores, NEG_BIG)
    block_peak = jnp.max(scores, axis=-1)
    weights = jnp.where(allowed[None], jnp.exp(scores - block_peak[..., None]), 0.0)
    block_total = jnp.sum(weights, axis=-1)
    weights16 = weights.astype(jnp.bfloat16)
    block_sum = jnp.einsum("hqk,khv->hqv", weights16, values, preferred_element_type=jnp.float32)
    return (block_peak, block_total, block_sum)


def merge_terms(earlier, later_part):
    top = jnp.maximum(earlier[0], later_part[0])
    old_factor = jnp.exp(earlier[0] - top)
    new_factor = jnp.exp(later_part[0] - top)
    return (
        top,
        earlier[1] * old_factor + later_part[1] * new_factor,
        earlier[2] * old_factor[..., None] + later_part[2] * new_factor[..., None],
    )


def chain_step(earlier, later_part):
    return (earlier[0] * later_part[0], later_part[0][..., None] * earlier[1] + later_part[1])


def shards(
    hidden_in,
    w_query_rec,
    w_forget,
    w_input,
    forget_gap,
    decay_extra,
    rec_gain,
    w_q_down,
    w_kv_down,
    w_key_rope,
    q_gain,
    kv_gain,
    w_q_nope,
    w_q_rope,
    w_k_up,
    w_v_up,
    w_out_rec,
    w_out_att,
):
    tok_dev = hidden_in.shape[0]
    sp_index = lax.axis_index("sp")
    tp_index = lax.axis_index("tp")
    full_query, full_forget, full_input = (
        lax.all_gather(w_query_rec, "sp", axis=0, tiled=True),
        lax.all_gather(w_forget, "sp", axis=0, tiled=True),
        lax.all_gather(w_input, "sp", axis=0, tiled=True),
    )
    left_weight = jnp.concatenate([full_query, full_forget, full_input], axis=1)
    right_weight = jnp.concatenate([w_q_down, w_kv_down, w_key_rope], axis=1)
    feature_piece = lax.all_gather(hidden_in, "tp", axis=1, tiled=True)
    left_sum = jnp.dot(feature_piece, left_weight, preferred_element_type=jnp.float32)
    right_sum = jnp.dot(feature_piece, right_weight, preferred_element_type=jnp.float32)
    key_cols = full_query.shape[1]
    head_count = key_cols // HG_KDIM
    left_round = left_sum.astype(jnp.bfloat16)
    rec_query = left_round[:, :key_cols].astype(jnp.float32).reshape(tok_dev, head_count, HG_KDIM)
    forget_pre = (
        left_round[:, key_cols : 2 * key_cols]
        .astype(jnp.float32)
        .reshape(tok_dev, head_count, HG_KDIM)
    )
    rec_value = (
        left_round[:, 2 * key_cols :].astype(jnp.float32).reshape(tok_dev, head_count, HG_VDIM)
    )
    gap_rows = forget_gap.reshape(head_count, HG_KDIM)
    closing = jax.nn.sigmoid(-forget_pre)
    key_in = gap_rows * closing
    log_forget = jnp.log1p(-gap_rows * closing) + decay_extra[:, :, None]
    block_count = tok_dev // HG_BLOCK

    def to_blocks(tensor):
        return tensor.reshape(block_count, HG_BLOCK, head_count, tensor.shape[-1]).transpose(
            0, 2, 1, 3
        )

    zero_state = jnp.zeros((head_count, HG_KDIM, HG_VDIM), jnp.float32)
    local_state, local_out = lax.scan(
        block_step,
        zero_state,
        (to_blocks(rec_query), to_blocks(key_in), to_blocks(rec_value), to_blocks(log_forget)),
    )
    local_out = local_out.transpose(0, 2, 1, 3).reshape(tok_dev, head_count, HG_VDIM)
    cumulative = jnp.cumsum(log_forget, axis=0)
    device_decay = jnp.exp(cumulative[-1])
    scanned = carried_in(
        (device_decay, local_state),
        "sp",
        chain_step,
        (jnp.ones_like(device_decay), jnp.zeros_like(local_state)),
    )
    into_state = scanned[1]
    rec_raw = local_out + jnp.einsum(
        "thd,hdv->thv", rec_query * jnp.exp(cumulative), into_state, precision=lax.Precision.HIGHEST
    )
    rec_out = (
        (rms_scale(rec_raw) * rec_gain).astype(jnp.bfloat16).reshape(tok_dev, head_count * HG_VDIM)
    )
    q_cols = w_q_down.shape[1]
    kv_cols = w_kv_down.shape[1]
    right_round = right_sum.astype(jnp.bfloat16)
    q_part = right_round[:, :q_cols]
    kv_part = right_round[:, q_cols : q_cols + kv_cols]
    rope_raw = right_sum[:, q_cols + kv_cols :]
    q_part32 = q_part.astype(jnp.float32)
    kv_part32 = kv_part.astype(jnp.float32)
    square_sums = lax.psum(
        (jnp.sum(q_part32 * q_part32, axis=1), jnp.sum(kv_part32 * kv_part32, axis=1)), "tp"
    )
    q_gain_part = lax.dynamic_slice_in_dim(q_gain, tp_index * q_cols, q_cols, 0)
    kv_gain_part = lax.dynamic_slice_in_dim(kv_gain, tp_index * kv_cols, kv_cols, 0)
    q_norm_part = (
        q_part32 * lax.rsqrt(square_sums[0][:, None] / q_gain.shape[0] + NORM_EPS) * q_gain_part
    ).astype(jnp.bfloat16)
    kv_norm_part = (
        kv_part32 * lax.rsqrt(square_sums[1][:, None] / kv_gain.shape[0] + NORM_EPS) * kv_gain_part
    ).astype(jnp.bfloat16)
    q_normed, latent = (
        lax.all_gather(q_norm_part, "tp", axis=1, tiled=True),
        lax.all_gather(kv_norm_part, "tp", axis=1, tiled=True),
    )
    q_start = sp_index * tok_dev
    cosine, sine_table = rotary_tables(tok_dev, q_start.astype(jnp.float32), ROPE)
    key_rope = rotate_half(rope_raw, cosine, sine_table).astype(jnp.bfloat16)
    att_heads = w_q_nope.shape[1] // NOPE
    q_nope = jnp.dot(q_normed, w_q_nope, preferred_element_type=jnp.float32).astype(jnp.bfloat16)
    q_nope = q_nope.reshape(tok_dev, att_heads, NOPE)
    q_rope = jnp.dot(q_normed, w_q_rope, preferred_element_type=jnp.float32).reshape(
        tok_dev, att_heads, ROPE
    )
    q_rope = rotate_half(q_rope, cosine[:, None, :], sine_table[:, None, :]).astype(jnp.bfloat16)

    def attend(running, latent_rows, rope_rows, key_start):

        def compute(previous):
            k_nope = jnp.dot(latent_rows, w_k_up, preferred_element_type=jnp.float32).astype(
                jnp.bfloat16
            )
            att_value = jnp.dot(latent_rows, w_v_up, preferred_element_type=jnp.float32).astype(
                jnp.bfloat16
            )
            partials = score_block(
                q_nope,
                q_rope,
                k_nope.reshape(-1, att_heads, NOPE),
                rope_rows,
                att_value.reshape(-1, att_heads, MLA_V),
                q_start,
                key_start,
            )
            return merge_terms(previous, partials)

        return lax.cond(key_start <= q_start, compute, lambda previous: previous, running)

    initial_att = (
        jnp.full((att_heads, tok_dev), NEG_BIG, jnp.float32),
        jnp.zeros((att_heads, tok_dev), jnp.float32),
        jnp.zeros((att_heads, tok_dev, MLA_V), jnp.float32),
    )
    latent_piece = lax.all_gather(latent, "sp", axis=0, tiled=True)
    rope_piece = lax.all_gather(key_rope, "sp", axis=0, tiled=True)

    def visit(block_index, current):
        first_row = block_index * tok_dev
        return attend(
            current,
            lax.dynamic_slice_in_dim(latent_piece, first_row, tok_dev, 0),
            lax.dynamic_slice_in_dim(rope_piece, first_row, tok_dev, 0),
            first_row,
        )

    top, total_w, accum = lax.fori_loop(0, latent_piece.shape[0] // tok_dev, visit, initial_att)
    att_out = (accum / total_w[..., None]).transpose(1, 0, 2).reshape(tok_dev, att_heads * MLA_V)
    att_out = att_out.astype(jnp.bfloat16)
    return lax.psum_scatter(
        (
            jnp.dot(rec_out, w_out_rec, preferred_element_type=jnp.float32)
            + jnp.dot(att_out, w_out_att, preferred_element_type=jnp.float32)
        ).astype(jnp.bfloat16),
        "tp",
        scatter_dimension=0,
        tiled=True,
    )


def solution(mesh):
    placed = (
        P("sp", "tp"),
        P("sp", "tp"),
        P("sp", "tp"),
        P("sp", "tp"),
        P("tp"),
        P("sp", "tp"),
        P(),
        P(None, "tp"),
        P(None, "tp"),
        P(),
        P(),
        P(),
        P(None, "tp"),
        P(None, "tp"),
        P(None, "tp"),
        P(None, "tp"),
        P("tp", None),
        P("tp", None),
    )
    return jax.shard_map(
        shards, mesh=mesh, in_specs=placed, out_specs=P(("sp", "tp"), None), check_vma=False
    )
```

profile of v0, /device:TPU:31, one launch (start us, length us, event | category | flops | bytes accessed | tf_op | source)
XLA Modules:
  0.0 697.5 jit_solution(387113204665993834)
XLA Ops:
  11.5 8.1 %all-gather.14.cloned.1.call-done = bf16[256,2048]{1,0:T(8,128)(2,1)} async-done(((bf16[256,1024]{1,0:T(8,128)(2,1)}), bf16[256,2048]{1,0:T(8,128)(2,1)}) %all-gather.14.cloned.1.call-update) | async-done | bytes 1048592 | tf_op jit(solution)/shard_map/all_gather | solution.py:146
  19.6 3.2 fusion.75
  22.9 3.0 all-reduce
  26.0 2.0 all_gather.41
  28.1 67.2 %all-gather.8.cloned.1.call-done = bf16[2048,1024]{1,0:T(8,128)(2,1)} async-done(((bf16[128,1024]{1,0:T(8,128)(2,1)}), bf16[2048,1024]{1,0:T(8,128)(2,1)}) %all-gather.8.cloned.1.call-update) | async-done | bytes 4194320 | tf_op jit(solution)/shard_map/all_gather | solution.py:140
  95.4 77.0 %all-gather.10.cloned.1.call-done = bf16[2048,1024]{1,0:T(8,128)(2,1)} async-done(((bf16[128,1024]{1,0:T(8,128)(2,1)}), bf16[2048,1024]{1,0:T(8,128)(2,1)}) %all-gather.10.cloned.1.call-update) | async-done | bytes 4194320 | tf_op jit(solution)/shard_map/all_gather | solution.py:141
  172.4 76.8 %all-gather.12.cloned.1.call-done = bf16[2048,1024]{1,0:T(8,128)(2,1)} async-done(((bf16[128,1024]{1,0:T(8,128)(2,1)}), bf16[2048,1024]{1,0:T(8,128)(2,1)}) %all-gather.12.cloned.1.call-update) | async-done | bytes 4194320 | tf_op jit(solution)/shard_map/all_gather | solution.py:142
  249.2 6.9 fusion.43
  257.4 1.5 slice_convert_fusion
  258.9 2.5 copy.75
  261.5 2.4 copy.106
  263.9 2.5 copy.76
  266.4 2.4 copy.107
  268.8 2.5 copy.73
  271.4 1.6 copy.105
  274.7 1.8 fusion.60
  276.5 164.5 %while.44 = (s32[]{:T(128)}, f32[8,128,128]{2,1,0:T(8,128)S(1)}, f32[4,8,64,128]{3,1,2,0:T(8,128)}, f32[4,8,64,128]{3,1,2,0:T(8,128)}, f32[4,8,64,128]{3,1,2,0:T...) while((s32[]{:T(128)}, f32[8,128,128]{2,1,0:T(8,128)S(1)}, ...), condition=%wide.region_2.3_spmd.clone, body=%wide.region_0.2_spmd.clone.sunk | while | flops 323690496 | bytes 42786940 | solution.py:173
  280.1 3.6 multiply_multiply_fusion.2
  283.7 30.8 %fusion.122 = f32[8,64,1,64]{3,2,1,0:T(1,128)S(1)} fusion(f32[8,64,64,128]{3,2,1,0:T(8,128)S(1)} %multiply_multiply_fusion.2, f32[8,64,128,1]{2,0,1,3:T(8,128)S(1)} %get-tuple-element.728), kind=kOutput, calls=%fused_computation.29.clone.1 | convolution fusion | flops 50331648 | bytes 17170432 | tf_op jit(solution)/shard_map/while/body/eval_jaxpr/htsd,hsd->hts/dot_general | solution.py:65
  321.1 3.6 multiply_multiply_fusion.2
  324.8 30.8 %fusion.122 = f32[8,64,1,64]{3,2,1,0:T(1,128)S(1)} fusion(f32[8,64,64,128]{3,2,1,0:T(8,128)S(1)} %multiply_multiply_fusion.2, f32[8,64,128,1]{2,0,1,3:T(8,128)S(1)} %get-tuple-element.728), kind=kOutput, calls=%fused_computation.29.clone.1 | convolution fusion | flops 50331648 | bytes 17170432 | tf_op jit(solution)/shard_map/while/body/eval_jaxpr/htsd,hsd->hts/dot_general | solution.py:65
  362.2 3.6 multiply_multiply_fusion.2
  365.8 30.8 %fusion.122 = f32[8,64,1,64]{3,2,1,0:T(1,128)S(1)} fusion(f32[8,64,64,128]{3,2,1,0:T(8,128)S(1)} %multiply_multiply_fusion.2, f32[8,64,128,1]{2,0,1,3:T(8,128)S(1)} %get-tuple-element.728), kind=kOutput, calls=%fused_computation.29.clone.1 | convolution fusion | flops 50331648 | bytes 17170432 | tf_op jit(solution)/shard_map/while/body/eval_jaxpr/htsd,hsd->hts/dot_general | solution.py:65
  403.3 3.6 multiply_multiply_fusion.2
  406.9 30.8 %fusion.122 = f32[8,64,1,64]{3,2,1,0:T(1,128)S(1)} fusion(f32[8,64,64,128]{3,2,1,0:T(8,128)S(1)} %multiply_multiply_fusion.2, f32[8,64,128,1]{2,0,1,3:T(8,128)S(1)} %get-tuple-element.728), kind=kOutput, calls=%fused_computation.29.clone.1 | convolution fusion | flops 50331648 | bytes 17170432 | tf_op jit(solution)/shard_map/while/body/eval_jaxpr/htsd,hsd->hts/dot_general | solution.py:65
  442.2 3.1 all_gather.43
  449.3 34.5 %all_gather.44 = bf16[4096,32]{0,1:T(8,128)(2,1)} all-gather(bf16[256,32]{0,1:T(8,128)(2,1)S(1)} %pad_maximum_fusion.1), channel_id=1, replica_groups=mesh['sp'=16,'tp'=2] {'sp'}, dimensions={0}, use_global_device_ids=true | all-gather | bytes 278528 | tf_op jit(solution)/shard_map/all_gather | solution.py:256
  483.8 4.1 copy.90
  487.9 108.1 %while.43 = (s32[]{:T(128)}, f32[8,256]{1,0:T(8,128)S(1)}, f32[8,256]{1,0:T(8,128)S(1)}, f32[8,256,64]{1,2,0:T(8,128)S(1)}, s32[]{:T(128)}, /*index=5*/bf16[4096...) while((s32[]{:T(128)}, f32[8,256]{1,0:T(8,128)S(1)}, ...), condition=%wide.region_17.18_spmd, body=%wide.region_12.17_spmd.sunk | while | flops 307962368 | bytes 15733113 | solution.py:267
  488.0 6.7 conditional.2
  490.9 1.5 fusion.76
  494.7 6.7 conditional.2
  501.5 6.7 conditional.2
  504.4 1.5 fusion.76
  508.2 6.8 conditional.2
  511.3 1.5 fusion.76
  515.1 6.7 conditional.2
  518.1 1.5 fusion.76
  521.9 6.7 conditional.2
  524.8 1.5 fusion.76
  528.6 6.7 conditional.2
  531.6 1.5 fusion.76
  535.4 6.7 conditional.2
  538.3 1.5 fusion.76
  542.1 6.7 conditional.2
  545.1 1.5 fusion.76
  548.9 6.7 conditional.2
  555.6 6.7 conditional.2
  562.4 6.7 conditional.2
  569.1 6.7 conditional.2
  575.9 6.7 conditional.2
  582.6 6.7 conditional.2
  589.3 6.7 conditional.2
  596.1 2.1 fusion.64
  598.2 1.7 copy.81
  601.4 1.6 copy.82
  603.0 2.1 slice.61
  606.4 2.7 copy.87
  609.1 28.6 %all_gather.38 = f32[16,8,128]{2,1,0:T(8,128)S(1)} all-gather(f32[1,8,128]{2,1,0:T(8,128)S(1)} %exp.49), channel_id=1, replica_groups=mesh['sp'=16,'tp'=2] {'sp'}, dimensions={0}, use_global_device_ids=true | all-gather | bytes 69632 | tf_op jit(solution)/shard_map/all_gather | solution.py:23
  637.6 2.9 copy_multiply_fusion
  640.5 20.3 %while.42 = (s32[]{:T(128)}, f32[8,128,128]{2,1,0:T(8,128)S(1)}, s32[]{:T(128)}, f32[16,8,128]{2,1,0:T(8,128)S(1)}, f32[16,8,128,128]{3,2,1,0:T(8,128)}, /*index=5*/s32[]{:T(128)}, s32[]{:T(128)}, s32[]{:T(128)}) while((s32[]{:T(128)}, f32[8,128,128]{2,1,0:T(8,128)S(1)}, s32[]{:T(128)}, f32[16,8,128]{2,1,0:T(8,128)S(1)}, ...), condition=%wide.region_6.7_spmd, body=%wide.region_5.6_spmd.sunk | while | flops 262149 | bytes 1585287 | solution.py:31
  660.9 3.0 multiply_reduce_fusion
  665.4 1.7 fusion.46
  667.2 23.5 %reduce-scatter.2.cloned.1.call-done = bf16[128,2048]{1,0:T(8,128)(2,1)} async-done(((bf16[256,2048]{1,0:T(8,128)(2,1)}), bf16[128,2048]{1,0:T(8,128)(2,1)}) %reduce-scatter.2.cloned.1.call-update) | async-done | bytes 524304 | tf_op jit(solution)/shard_map/reduce_scatter | solution.py:270
  (361 shorter events, 157.8 us)
Async XLA Ops:
  6.5 658.9 %copy-start = (bf16[512,2048]{1,0:T(8,128)(2,1)S(1)}, bf16[512,2048]{1,0:T(8,128)(2,1)}, u32[]{:S(2)}) copy-start(bf16[512,2048]{1,0:T(8,128)(2,1)} %param.43) | copy-start | bytes 6291460
  6.5 4.9 copy-start.14
  6.5 5.0 copy-start.9
  6.5 13.0 %all-gather.14.cloned.1.call-start = ((), (), s32[]{:S(2)}) async-start(), calls=%async_computation.4 | async-start | bytes 1572864 | tf_op jit(solution)/shard_map/all_gather | solution.py:146
  7.3 88.1 %all-gather.8.cloned.1.call-start = ((), (), s32[]{:S(2)}) async-start(), calls=%async_computation.1 | async-start | bytes 4456448 | tf_op jit(solution)/shard_map/all_gather | solution.py:140
  8.0 164.3 %all-gather.10.cloned.1.call-start = ((), (), s32[]{:S(2)}) async-start(), calls=%async_computation.2 | async-start | bytes 4456448 | tf_op jit(solution)/shard_map/all_gather | solution.py:141
  8.7 240.5 %all-gather.12.cloned.1.call-start = ((), (), s32[]{:S(2)}) async-start(), calls=%async_computation.3 | async-start | bytes 4456448 | tf_op jit(solution)/shard_map/all_gather | solution.py:142
  9.3 474.5 %all-gather.16.cloned.1.call-start = ((), (), s32[]{:S(2)}) async-start(), calls=%async_computation.5 | async-start | bytes 2228224 | tf_op jit(solution)/shard_map/all_gather | solution.py:255
  11.5 263.2 %copy-start.7 = (f32[8,128]{1,0:T(8,128)}, f32[8,128]{1,0:T(8,128)S(1)}, u32[]{:S(2)}) copy-start(f32[8,128]{1,0:T(8,128)S(1)} %bitcast_negate_fusion) | copy-start | bytes 12292
  28.1 612.4 %all-gather.18.cloned.1.call-start = ((), (), s32[]{:S(2)}) async-start(), calls=%async_computation.7 | async-start | bytes 8912896 | tf_op jit(solution)/shard_map/all_gather | solution.py:23
  271.4 1.6 copy-start.4
  271.4 1.9 copy-start.5
  276.5 165.4 %copy-start.8 = (f32[8,128]{1,0:T(8,128)S(1)}, f32[8,128]{1,0:T(8,128)}, u32[]{:S(2)}) copy-start(f32[8,128]{1,0:T(8,128)} %copy-done.7) | copy-start | bytes 12292
  276.5 165.5 %copy-start.12 = (f32[512]{0:T(512)S(1)}, f32[512]{0:T(512)}, u32[]{:S(2)}) copy-start(f32[512]{0:T(512)} %param.36) | copy-start | bytes 6148
  276.5 165.6 %copy-start.10 = (f32[256]{0:T(256)S(1)}, f32[256]{0:T(256)}, u32[]{:S(2)}) copy-start(f32[256]{0:T(256)} %get-tuple-element.540) | copy-start | bytes 3076
  276.5 168.8 %copy-start.6 = (bf16[512,512]{1,0:T(8,128)(2,1)S(1)}, bf16[512,512]{1,0:T(8,128)(2,1)}, u32[]{:S(2)}) copy-start(bf16[512,512]{1,0:T(8,128)(2,1)} %param.38) | copy-start | bytes 1572868
  441.0 0.8 copy-start.1
  441.8 248.9 %reduce-scatter.2.cloned.1.call-start = ((), (), s32[]{:S(2)}) async-start(), calls=%async_computation.6 | async-start | bytes 1572864 | tf_op jit(solution)/shard_map/reduce_scatter | solution.py:270
  490.9 1.5 copy-start.3
  497.7 1.5 copy-start.3
  504.4 1.5 copy-start.3
  511.3 1.5 copy-start.3
  518.1 1.5 copy-start.3
  524.8 1.5 copy-start.3
  531.6 1.5 copy-start.3
  538.3 1.5 copy-start.3
  545.1 1.5 copy-start.3
  551.8 1.5 copy-start.3
  558.6 1.5 copy-start.3
  565.3 1.5 copy-start.3
  572.0 1.5 copy-start.3
  578.8 1.5 copy-start.3
  585.5 1.5 copy-start.3
  592.3 1.5 copy-start.3
  603.0 34.6 %copy-start.2 = (f32[256,1024]{0,1:T(8,128)S(1)}, f32[256,1024]{0,1:T(8,128)}, u32[]{:S(2)}) copy-start(f32[256,1024]{0,1:T(8,128)} %get-tuple-element.554) | copy-start | bytes 3145732
  660.9 3.1 copy-start.11
  660.9 3.2 copy-start.13
Sparse Core Ops, SparseCore 0:
  8.9 10.6 all-gather.13
  22.3 72.9 all-gather.7
  98.1 74.1 all-gather.9
  175.0 74.1 all-gather.11
  251.8 63.3 all-gather.15
  441.9 113.2 all-gather.17
  667.3 23.3 reduce-scatter.1
where the time goes:
time: 702 us; the launch traced here: 698 us
  waiting for transfers between devices  255 us (36%)
  matrix products  244 us (35%)
  blocking collectives  71.2 us (10%)
  other arithmetic  63.9 us (9%)
  local copies, waits for them, and re-layouts  45.9 us (7%)
  between operations  13.8 us (2%)
    dot_general x4, matrix products, block_step(): jnp.einsum('htsd,hsd->hts', queries[:, :, None, :] * decays, key_in, prec...  123 us
    all_gather x1, waiting for transfers between devices, shards(): lax.all_gather(w_forget, 'sp', axis=0, tiled=True)  77 us
    all_gather x1, waiting for transfers between devices, shards(): lax.all_gather(w_input, 'sp', axis=0, tiled=True)  76.8 us
    all_gather x1, waiting for transfers between devices, shards(): lax.all_gather(w_query_rec, 'sp', axis=0, tiled=True)  67.2 us
    all_gather x1, blocking collectives, shards(): rope_piece = lax.all_gather(key_rope, 'sp', axis=0, tiled=True)  34.5 us
    all_gather x1, blocking collectives, carried_in(): gathered = jax.tree.map(lambda a: lax.all_gather(a, axis), part)  28.6 us
    reduce_scatter x1, waiting for transfers between devices, shards(): lax.psum_scatter((jnp.dot(rec_out, w_out_rec, preferred_element_type=jnp....  23.5 us
    dot_general x16, matrix products, score_block(): jnp.einsum('qhd,khd->hqk', q_nope, k_nope, preferred_element_type=jnp.flo...  23.5 us
  transfers between devices with their start and end apart: 7, of which 5 were waited for; matrix products, arithmetic and copies ran while one was open for 47% of the time, Pallas kernels for 0%

commit v1 on v0

v1 whole, which is shorter than its diff:
```python
import math

import jax
import jax.numpy as jnp
from jax import lax
from jax.experimental import pallas as pl
from jax.experimental.pallas import tpu as pltpu
from jax.sharding import Mesh
from jax.sharding import PartitionSpec as P

HG_KDIM = 128
HG_VDIM = 128
HG_BLOCK = 64
NOPE = 64
ROPE = 32
MLA_V = 64


NORM_EPS = 1e-06
ROPE_BASE = 10000.0
NEG_BIG = -1e30


def rotate_half(values, cosine, sine_table):
    half_width = values.shape[-1] // 2
    lower_half = values[..., :half_width]
    upper_half = values[..., half_width:]
    return jnp.concatenate(
        [
            lower_half * cosine - upper_half * sine_table,
            lower_half * sine_table + upper_half * cosine,
        ],
        axis=-1,
    )


def rotary_tables(row_count, offset, rot_width):
    positions = jnp.arange(row_count, dtype=jnp.float32) + offset
    frequency = 1.0 / ROPE_BASE ** (jnp.arange(0, rot_width, 2, dtype=jnp.float32) / rot_width)
    angles = positions[:, None] * frequency[None, :]
    return (jnp.cos(angles), jnp.sin(angles))


def dot_t(left, right, left_dim, right_dim):
    return lax.dot_general(
        left, right, (((left_dim,), (right_dim,)), ((), ())), preferred_element_type=jnp.float32
    )


def recurrence_body(rows, q_ref, k_ref, v_ref, lf_ref, s_ref, gain_ref, out_ref, state_ref):
    row_id = lax.broadcasted_iota(jnp.int32, (rows, rows), 0)
    col_id = lax.broadcasted_iota(jnp.int32, (rows, rows), 1)
    lower = row_id >= col_id
    ones = jnp.where(lower, 1.0, 0.0).astype(jnp.float32)
    state = s_ref[0]
    for step in range(k_ref.shape[0] // rows):
        here = pl.ds(step * rows, rows)
        cumulative = jnp.dot(
            ones,
            lf_ref[here, :],
            precision=lax.Precision.HIGHEST,
            preferred_element_type=jnp.float32,
        )
        last = cumulative[rows - 1 : rows, :]
        keys = k_ref[here, :]
        values = v_ref[here, :]
        if out_ref is not None:
            centre = cumulative[rows // 2 - 1 : rows // 2, :]
            queries = q_ref[here, :].astype(jnp.float32)
            q_mid = (queries * jnp.exp(cumulative - centre)).astype(jnp.bfloat16)
            k_mid = (keys * jnp.exp(centre - cumulative)).astype(jnp.bfloat16)
            scores = jnp.where(lower, dot_t(q_mid, k_mid, 1, 1), 0.0).astype(jnp.bfloat16)
            raw = dot_t(scores, values, 1, 0) + dot_t(
                (queries * jnp.exp(cumulative)).astype(jnp.bfloat16),
                state.astype(jnp.bfloat16),
                1,
                1,
            )
            scale = lax.rsqrt(jnp.mean(raw * raw, axis=-1, keepdims=True) + NORM_EPS)
            out_ref[here, :] = (raw * scale * gain_ref[...]).astype(jnp.bfloat16)
        k_last = (keys * jnp.exp(last - cumulative)).astype(jnp.bfloat16)
        state = jnp.exp(last) * state + dot_t(values, k_last, 0, 0)
    if state_ref is not None:
        state_ref[0] = state


def recurrence(queries, keys, values, log_forget, state, gain, emit):
    tokens, width = keys.shape
    heads = width // HG_KDIM
    rows = 2 * HG_BLOCK

    def body(q_ref, k_ref, v_ref, lf_ref, s_ref, gain_ref, out_ref):
        recurrence_body(
            rows,
            q_ref,
            k_ref,
            v_ref,
            lf_ref,
            s_ref,
            gain_ref,
            out_ref if emit else None,
            None if emit else out_ref,
        )

    column = pl.BlockSpec((tokens, HG_KDIM), lambda h: (0, h))
    one_state = pl.BlockSpec((1, HG_VDIM, HG_KDIM), lambda h: (h, 0, 0))
    return pl.pallas_call(
        body,
        grid=(heads,),
        in_specs=[
            column,
            column,
            column,
            column,
            one_state,
            pl.BlockSpec((1, HG_VDIM), lambda h: (0, 0)),
        ],
        out_specs=column if emit else one_state,
        out_shape=jax.ShapeDtypeStruct((tokens, width), jnp.bfloat16)
        if emit
        else jax.ShapeDtypeStruct(state.shape, jnp.float32),
        compiler_params=pltpu.CompilerParams(vmem_limit_bytes=32 * 1024 * 1024),
        cost_estimate=pl.CostEstimate(
            flops=tokens * width * 4000, bytes_accessed=tokens * width * 14, transcendentals=0
        ),
        name="rec_out" if emit else "rec_state",
    )(queries, keys, values, log_forget, state, gain)


def attention_body(
    heads, at_ref, q_ref, lat_ref, rope_ref, wk_ref, wv_ref, out_ref, top_ref, tot_ref, acc_ref
):
    step = pl.program_id(0)
    mine = at_ref[0]

    @pl.when(step == 0)
    def _():
        top_ref[...] = jnp.full(top_ref.shape, NEG_BIG, jnp.float32)
        tot_ref[...] = jnp.zeros(tot_ref.shape, jnp.float32)
        acc_ref[...] = jnp.zeros(acc_ref.shape, jnp.float32)

    def visit(masked):
        latent = lat_ref[...]
        rope = rope_ref[...]
        k_all = dot_t(wk_ref[...], latent, 1, 1).astype(jnp.bfloat16)
        v_all = dot_t(wv_ref[...], latent, 1, 1).astype(jnp.bfloat16)
        for head in range(heads):
            k_head = jnp.concatenate([k_all[head * NOPE : (head + 1) * NOPE], rope], axis=0)
            scores = dot_t(k_head, q_ref[head], 0, 0) * (1.0 / math.sqrt(NOPE + ROPE))
            if masked:
                key_id = lax.broadcasted_iota(jnp.int32, scores.shape, 0)
                query_id = lax.broadcasted_iota(jnp.int32, scores.shape, 1)
                scores = jnp.where(key_id <= query_id, scores, NEG_BIG)
            peak = jnp.max(scores, axis=0, keepdims=True)
            weights = jnp.exp(scores - peak)
            total = jnp.sum(weights, axis=0, keepdims=True)
            part = dot_t(
                v_all[head * MLA_V : (head + 1) * MLA_V], weights.astype(jnp.bfloat16), 1, 0
            )
            before = top_ref[head]
            top = jnp.maximum(before, peak)
            old = jnp.exp(before - top)
            new = jnp.exp(peak - top)
            top_ref[head] = top
            tot_ref[head] = tot_ref[head] * old + total * new
            acc_ref[head] = acc_ref[head] * old + part * new

    @pl.when(step < mine)
    def _():
        visit(False)

    @pl.when(step == mine)
    def _():
        visit(True)
        for head in range(heads):
            out_ref[head * MLA_V : (head + 1) * MLA_V, :] = (
                acc_ref[head] / tot_ref[head]
            ).astype(jnp.bfloat16)


def attention(place, queries, latent, rope, w_key, w_value):
    heads, width, rows = queries.shape
    blocks = latent.shape[0] // rows
    grid_spec = pltpu.PrefetchScalarGridSpec(
        num_scalar_prefetch=1,
        grid=(blocks,),
        in_specs=[
            pl.BlockSpec((heads, width, rows), lambda i, at: (0, 0, 0)),
            pl.BlockSpec((rows, latent.shape[1]), lambda i, at: (jnp.minimum(i, at[0]), 0)),
            pl.BlockSpec((rope.shape[0], rows), lambda i, at: (0, jnp.minimum(i, at[0]))),
            pl.BlockSpec(w_key.shape, lambda i, at: (0, 0)),
            pl.BlockSpec(w_value.shape, lambda i, at: (0, 0)),
        ],
        out_specs=pl.BlockSpec((heads * MLA_V, rows), lambda i, at: (0, 0)),
        scratch_shapes=[
            pltpu.VMEM((heads, 1, rows), jnp.float32),
            pltpu.VMEM((heads, 1, rows), jnp.float32),
            pltpu.VMEM((heads, MLA_V, rows), jnp.float32),
        ],
    )

    def body(*refs):
        attention_body(heads, *refs)

    return pl.pallas_call(
        body,
        grid_spec=grid_spec,
        out_shape=jax.ShapeDtypeStruct((heads * MLA_V, rows), jnp.bfloat16),
        compiler_params=pltpu.CompilerParams(
            dimension_semantics=("arbitrary",), vmem_limit_bytes=32 * 1024 * 1024
        ),
        cost_estimate=pl.CostEstimate(
            flops=blocks * heads * rows * rows * 2000,
            bytes_accessed=latent.size * 2,
            transcendentals=0,
        ),
        name="attend",
    )(place, queries, latent, rope, w_key, w_value)


def both_halves(part, axis):
    if lax.axis_size("tp") != 2:
        return lax.all_gather(part, "tp", axis=axis, tiled=True)
    other = lax.ppermute(part, "tp", [(0, 1), (1, 0)])
    first = lax.axis_index("tp") == 0
    return jnp.concatenate(
        [jnp.where(first, part, other), jnp.where(first, other, part)], axis=axis
    )


def shards(
    hidden_in,
    w_query_rec,
    w_forget,
    w_input,
    forget_gap,
    decay_extra,
    rec_gain,
    w_q_down,
    w_kv_down,
    w_key_rope,
    q_gain,
    kv_gain,
    w_q_nope,
    w_q_rope,
    w_k_up,
    w_v_up,
    w_out_rec,
    w_out_att,
):
    tok_dev = hidden_in.shape[0]
    group = lax.axis_size("pl")
    pl_index = lax.axis_index("pl")
    zz_index = lax.axis_index("zz")
    tp_index = lax.axis_index("tp")
    tp_size = lax.axis_size("tp")
    sp_index = zz_index * group + pl_index

    cols = w_query_rec.shape[1] // group
    heads = cols // HG_KDIM
    depth = w_query_rec.shape[0]
    packed = jnp.concatenate(
        [w.reshape(depth, group, cols) for w in (w_query_rec, w_forget, w_input)], axis=2
    )
    swapped = lax.all_to_all(packed, "pl", split_axis=1, concat_axis=0, tiled=True)
    left_weight = lax.all_gather(
        swapped.reshape(group * depth, 3 * cols), "zz", axis=0, tiled=True
    )
    feature_piece = both_halves(hidden_in, 1)
    group_rows = both_halves(lax.all_gather(hidden_in, "pl", axis=0, tiled=True), 1)
    group_decay = lax.all_gather(decay_extra, "pl", axis=0, tiled=True)
    group_decay = lax.dynamic_slice_in_dim(group_decay, pl_index * heads, heads, 1)

    right_weight = jnp.concatenate([w_q_down, w_kv_down, w_key_rope], axis=1)
    right_sum = jnp.dot(feature_piece, right_weight, preferred_element_type=jnp.float32)
    q_cols = w_q_down.shape[1]
    kv_cols = w_kv_down.shape[1]
    right_round = right_sum[:, : q_cols + kv_cols].astype(jnp.bfloat16)
    both = both_halves(right_round[None], 0).astype(jnp.float32)
    q_latent = jnp.concatenate([both[i, :, :q_cols] for i in range(tp_size)], axis=1)
    kv_latent = jnp.concatenate([both[i, :, q_cols:] for i in range(tp_size)], axis=1)
    q_normed = (
        q_latent
        * lax.rsqrt(jnp.mean(q_latent * q_latent, axis=-1, keepdims=True) + NORM_EPS)
        * q_gain
    ).astype(jnp.bfloat16)
    latent = (
        kv_latent
        * lax.rsqrt(jnp.mean(kv_latent * kv_latent, axis=-1, keepdims=True) + NORM_EPS)
        * kv_gain
    ).astype(jnp.bfloat16)
    q_start = sp_index * tok_dev
    cosine, sine_table = rotary_tables(tok_dev, q_start.astype(jnp.float32), ROPE)
    key_rope = rotate_half(right_sum[:, q_cols + kv_cols :], cosine, sine_table).astype(
        jnp.bfloat16
    )
    keys_all = lax.all_gather(
        jnp.concatenate([latent, key_rope], axis=1), ("zz", "pl"), axis=0, tiled=True
    )
    att_heads = w_q_nope.shape[1] // NOPE
    q_nope = jnp.dot(q_normed, w_q_nope, preferred_element_type=jnp.float32).astype(jnp.bfloat16)
    q_rope = jnp.dot(q_normed, w_q_rope, preferred_element_type=jnp.float32).reshape(
        tok_dev, att_heads, ROPE
    )
    q_rope = rotate_half(q_rope, cosine[:, None, :], sine_table[:, None, :]).astype(jnp.bfloat16)
    queries = jnp.concatenate([q_nope.reshape(tok_dev, att_heads, NOPE), q_rope], axis=2)
    att_out = attention(
        sp_index.astype(jnp.int32).reshape(1),
        queries.transpose(1, 2, 0),
        keys_all[:, : latent.shape[1]],
        keys_all[:, latent.shape[1] :].T,
        w_k_up.T,
        w_v_up.T,
    )

    left_round = jnp.dot(
        group_rows, left_weight, preferred_element_type=jnp.float32
    ).astype(jnp.bfloat16)
    rec_query = left_round[:, :cols]
    rec_value = left_round[:, 2 * cols :]
    gap = lax.dynamic_slice_in_dim(forget_gap, pl_index * cols, cols, 0)
    key_in = gap * jax.nn.sigmoid(-left_round[:, cols : 2 * cols].astype(jnp.float32))
    log_forget = jnp.log1p(-key_in) + jnp.repeat(group_decay, HG_KDIM, axis=1)
    gain = rec_gain.reshape(1, HG_VDIM)
    zero_state = jnp.zeros((heads, HG_VDIM, HG_KDIM), jnp.float32)
    local_state = recurrence(rec_query, key_in, rec_value, log_forget, zero_state, gain, False)
    decay = jnp.exp(jnp.sum(log_forget, axis=0)).reshape(heads, 1, HG_KDIM)
    reached = lax.all_gather(jnp.concatenate([local_state, decay], axis=1), "zz", axis=0)
    into_state = zero_state
    for place in range(lax.axis_size("zz") - 1):
        later = reached[place, :, HG_VDIM:] * into_state + reached[place, :, :HG_VDIM]
        into_state = jnp.where(place < zz_index, later, into_state)
    group_out = recurrence(rec_query, key_in, rec_value, log_forget, into_state, gain, True)
    rec_out = lax.all_to_all(group_out, "pl", split_axis=0, concat_axis=1, tiled=True)

    mixed = jnp.dot(rec_out, w_out_rec, preferred_element_type=jnp.float32) + dot_t(
        att_out, w_out_att, 0, 0
    )
    if tp_size != 2:
        return lax.psum_scatter(
            mixed.astype(jnp.bfloat16), "tp", scatter_dimension=0, tiled=True
        )
    half = tok_dev // 2
    sent = lax.dynamic_slice_in_dim(mixed, (1 - tp_index) * half, half, 0).astype(jnp.bfloat16)
    kept = lax.dynamic_slice_in_dim(mixed, tp_index * half, half, 0)
    came = lax.ppermute(sent, "tp", [(0, 1), (1, 0)])
    return (kept + came.astype(jnp.float32)).astype(jnp.bfloat16)


def solution(mesh):
    placed = (
        P(("zz", "pl"), "tp"),
        P(("zz", "pl"), "tp"),
        P(("zz", "pl"), "tp"),
        P(("zz", "pl"), "tp"),
        P("tp"),
        P(("zz", "pl"), "tp"),
        P(),
        P(None, "tp"),
        P(None, "tp"),
        P(),
        P(),
        P(),
        P(None, "tp"),
        P(None, "tp"),
        P(None, "tp"),
        P(None, "tp"),
        P("tp", None),
        P("tp", None),
    )
    sp_size, tp_size = mesh.shape["sp"], mesh.shape["tp"]

    def run(hidden_in, w_query_rec, *rest):
        heads_dev = w_query_rec.shape[1] // HG_KDIM // tp_size
        group = math.gcd(math.gcd(heads_dev, 4), sp_size)
        split_mesh = Mesh(
            mesh.devices.reshape(sp_size // group, group, tp_size), ("zz", "pl", "tp")
        )
        return jax.shard_map(
            shards,
            mesh=split_mesh,
            in_specs=placed,
            out_specs=P(("zz", "pl", "tp"), None),
            check_vma=False,
        )(hidden_in, w_query_rec, *rest)

    return run
```

time: 702 us -> 287 us (0.41)
  matrix products: 244 us -> 15.4 us
  waiting for transfers between devices: 255 us -> 123 us
  other arithmetic: 63.9 us -> 11.6 us
  Pallas kernels: 0 us -> 50.6 us
  blocking collectives: 71.2 us -> 38.5 us
  local copies, waits for them, and re-layouts: 45.9 us -> 24.2 us
  starting transfers between devices: 0.24 us -> 9.12 us
    dot_general x99 -> x2, matrix products: 238 us -> 7.31 us  [the longest x1 6.56 us: shards(): jnp.dot(group_rows, left_weight, preferred_element_type=jnp.float32)]
    all_gather x6 -> x3, waiting for transfers between devices: 229 us -> 120 us  [the longest x1 61.6 us: shards(): lax.all_gather(jnp.concatenate([latent, key_rope], axis=1), ('zz', 'pl'),...]
    pallas_call x0 -> x3, Pallas kernels: none -> 50.6 us  [the longest x1 41.5 us: attention(): pl.pallas_call(body, grid_spec=grid_spec, out_shape=jax.ShapeDtypeStruct(...]
    all_gather x4 -> x2, blocking collectives: 68.2 us -> 20.2 us  [the longest x1 13.8 us: shards(): lax.all_gather(jnp.concatenate([local_state, decay], axis=1), 'zz', axis=0)]
    reduce_scatter x1 -> x0, waiting for transfers between devices: 23.5 us -> none  [shards(): lax.psum_scatter((jnp.dot(rec_out, w_out_rec, preferred_element_type=jnp....]
    mul x9 -> x0, other arithmetic: 21.9 us -> none  [the longest x4 14.5 us: block_step(): queries[:, :, None, :] * decays]
    add x47 -> x0, other arithmetic: 20 us -> none  [the longest x15 19.7 us: chain_step(): later_part[0][..., None] * earlier[1] + later_part[1]]
    all_to_all x0 -> x1, blocking collectives: none -> 18.3 us  [shards(): lax.all_to_all(packed, 'pl', split_axis=1, concat_axis=0, tiled=True)]
  transfers between devices with their start and end apart: 7 -> 8, of which waited for: 5 -> 6; matrix products, arithmetic and copies ran while one was open for 47% -> 11% of each run, Pallas kernels for 0% -> 15%
where the time goes in v1:
time: 287 us; the launch traced here: 286 us
  waiting for transfers between devices  123 us (43%)
  Pallas kernels  50.6 us (18%)
  blocking collectives  38.5 us (13%)
  local copies, waits for them, and re-layouts  24.2 us (8%)
  matrix products  15.4 us (5%)
  between operations  13.6 us (5%)
  other arithmetic  11.6 us (4%)
  starting transfers between devices  9.12 us (3%)
    all_gather x1, waiting for transfers between devices, shards(): lax.all_gather(jnp.concatenate([latent, key_rope], axis=1), ('zz', 'pl'),...  61.6 us
    all_gather x1, waiting for transfers between devices, shards(): lax.all_gather(swapped.reshape(group * depth, 3 * cols), 'zz', axis=0, ti...  50.8 us
    pallas_call x1, Pallas kernels, attention(): pl.pallas_call(body, grid_spec=grid_spec, out_shape=jax.ShapeDtypeStruct(...  41.5 us
    all_to_all x1, blocking collectives, shards(): lax.all_to_all(packed, 'pl', split_axis=1, concat_axis=0, tiled=True)  18.3 us
    all_gather x1, blocking collectives, shards(): lax.all_gather(jnp.concatenate([local_state, decay], axis=1), 'zz', axis=0)  13.8 us
    pallas_call x2, Pallas kernels, recurrence(): pl.pallas_call(body, grid=(heads,), in_specs=[column, column, column, col...  9.12 us
    all_gather x1, waiting for transfers between devices, shards(): lax.all_gather(hidden_in, 'pl', axis=0, tiled=True)  7.85 us
    unnamed x36, local copies, waits for them, and re-layouts  7.8 us
  transfers between devices with their start and end apart: 8, of which 6 were waited for; matrix products, arithmetic and copies ran while one was open for 11% of the time, Pallas kernels for 15%

profile of v1, /device:TPU:31, one launch (start us, length us, event | category | flops | bytes accessed | tf_op | source)
XLA Modules:
  0.0 286.2 jit_solution(4265769512496210441)
XLA Ops:
  6.5 0.7 all-gather.5.cloned.1.call-update
  7.3 0.0 all-gather.9.cloned.1.call-start
  7.3 0.7 collective-permute-start.1
  8.0 1.2 copy.49
  9.2 0.0 copy-start.13
  9.3 0.5 collective-permute-done.1
  9.8 1.1 broadcast_select_fusion.3
  10.9 0.9 fusion.4
  11.9 0.0 copy-start.12
  11.9 0.0 copy-start.8
  11.9 0.4 collective-permute-start.2
  12.4 0.7 subtract_convert_fusion.1
  13.1 0.3 collective-permute-done.2
  13.5 0.1 multiply_reduce_fusion.1
  13.6 0.1 multiply_convert_fusion.1
  13.7 0.7 pad_maximum_fusion.3
  14.4 0.0 all-gather.9.cloned.1.call-update
  14.4 0.0 all-gather.7.cloned.1.call-start
  14.5 0.2 copy.43
  14.7 0.2 copy.44
  14.8 0.2 copy.45
  15.0 0.1 pad_maximum_fusion
  15.1 18.3 %all_to_all.34 = bf16[128,4,768]{0,2,1:T(8,128)(2,1)S(1)} all-to-all(bf16[128,4,768]{0,2,1:T(8,128)(2,1)S(1)} %pad_maximum_fusion), channel_id=1, replica_groups=mesh['zz'=4,'pl'=4,'tp'=2] {'pl'}, dimensions={1} | all-to-all | bytes 1572864 | tf_op jit(solution)/shard_map/all_to_all | solution.py:265
  33.4 1.2 copy.46
  34.6 0.0 all-gather.7.cloned.1.call-update
  34.6 0.1 copy.51
  34.8 1.1 copy.52
  35.9 6.4 %all_gather.20 = f32[1024,8]{0,1:T(8,128)S(1)} all-gather(f32[256,8]{0,1:T(8,128)} %param.23), channel_id=1, replica_groups=mesh['zz'=4,'pl'=4,'tp'=2] {'pl'}, dimensions={0}, use_global_device_ids=true | all-gather | bytes 40960 | tf_op jit(solution)/shard_map/all_gather | solution.py:271
  42.3 1.0 copy.47
  43.3 0.8 dynamic_slice.12
  44.1 1.0 maximum_convert_fusion
  45.0 7.8 %all-gather.5.cloned.1.call-done = bf16[1024,1024]{1,0:T(8,128)(2,1)} async-done(((bf16[256,1024]{1,0:T(8,128)(2,1)}), bf16[1024,1024]{1,0:T(8,128)(2,1)}) %all-gather.5.cloned.1.call-update) | async-done | bytes 2097168 | tf_op jit(solution)/shard_map/all_gather | solution.py:270
  52.9 0.8 collective-permute-start
  53.7 1.1 slice_bitcast_fusion.2
  54.8 0.1 multiply_reduce_fusion
  54.9 2.2 convolution_convert_fusion
  57.0 1.1 copy.50
  58.1 1.3 fusion.25
  59.6 61.6 %all-gather.9.cloned.1.call-done = bf16[4096,288]{0,1:T(8,128)(2,1)} async-done(((bf16[256,288]{0,1:T(8,128)(2,1)}), bf16[4096,288]{0,1:T(8,128)(2,1)}) %all-gather.9.cloned.1.call-update) | async-done | bytes 2359312 | tf_op jit(solution)/shard_map/all_gather | solution.py:297
  121.1 3.2 %slice.100 = bf16[4096,256]{0,1:T(8,128)(2,1)} slice(bf16[4096,288]{0,1:T(8,128)(2,1)} %all-gather.9.cloned.1.call-done), slice={[0:4096], [0:256]} | slice | bytes 4194304 | tf_op jit(solution)/shard_map/slice | solution.py:310
  124.3 4.1 %copy.53.refs_2_ = bf16[4096,256]{1,0:T(8,128)(2,1)} copy(bf16[4096,256]{0,1:T(8,128)(2,1)} %slice.100) | data formatting | bytes 4194304 | tf_op jit(solution)/shard_map/slice | solution.py:310
  128.4 1.7 slice_bitcast_fusion.refs_3_
  130.0 4.8 %broadcast_select_fusion.1 = (bf16[1024,1024]{1,0:T(8,128)(2,1)}, bf16[1024,1024]{1,0:T(8,128)(2,1)}) fusion(bf16[1024,1024]{1,0:T(8,128)(2,1)} %all-gather.5.cloned.1.call-done, bf16[1024,1024]{1,0:T(8,128)(2,1)} %collective-permute-done, pred[]{:T(512)S(6)} %eq.2), kind=kLoop, calls=%fused_computation.12 | loop fusion | flops 2097152 | bytes 8388609 | tf_op jit(solution)/shard_map/jit(_where)/select_n | solution.py:227
  134.8 50.8 %all-gather.7.cloned.1.call-done = bf16[2048,768]{1,0:T(8,128)(2,1)} async-done(((bf16[512,768]{1,0:T(8,128)(2,1)}), bf16[2048,768]{1,0:T(8,128)(2,1)}) %all-gather.7.cloned.1.call-update) | async-done | bytes 3145744 | tf_op jit(solution)/shard_map/all_gather | solution.py:266
  185.6 6.6 %fusion.10 = bf16[1024,768]{1,0:T(8,128)(2,1)S(1)} fusion(bf16[2048,768]{1,0:T(8,128)(2,1)} %all-gather.7.cloned.1.call-done, bf16[1024,1024]{1,0:T(8,128)(2,1)} %get-tuple-element.8, bf16[1024,1024]{1,0:T(8,128)(2,1)} %get-tuple-element.7), kind=kOutput, calls=%fused_computation.13 | convolution fusion | flops 3230400512 | bytes 8912896 | tf_op jit(solution)/shard_map/dot_general | solution.py:316
  192.2 0.1 fusion.27
  192.3 1.0 copy-done.5
  193.2 1.2 broadcast_in_dim.8
  194.4 0.6 fusion.26
  195.1 4.7 %rec_state.1 = f32[2,128,128]{2,1,0:T(8,128)S(1)} custom-call(bf16[1024,256]{1,0:T(8,128)(2,1)S(1)} %get-tuple-element.11.q_ref, f32[1024,256]{1,0:T(8,128)S(1)} %get-tuple-element.9.k_ref, bf16[1024,256]{1,0:T(8,128)(2,1)S(1)} %get-tuple-element.10.v_ref, f32[1024,256]{1,0:T(8,128)S(1)} %get-tuple-element.6.lf_ref, ...), custom_call_target="tpu_custom_call" | custom-call | flops 1048576000 | bytes 3670016 | tf_op jit(solution)/shard_map/rec_state/pallas_call | solution.py:107
  199.9 13.8 %all-gather = f32[8,129,128]{2,1,0:T(8,128)S(1)} all-gather(f32[2,129,128]{2,1,0:T(8,128)S(1)} %pad_maximum_fusion.4), channel_id=2, replica_groups=mesh['zz'=4,'pl'=4,'tp'=2] {'zz'}, dimensions={0}, use_global_device_ids=true | all-gather | bytes 660480 | tf_op jit(solution)/shard_map/all_gather | solution.py:328
  213.7 4.4 %rec_out.1 = bf16[1024,256]{1,0:T(8,128)(2,1)S(1)} custom-call(bf16[1024,256]{1,0:T(8,128)(2,1)S(1)} %get-tuple-element.11.q_ref, f32[1024,256]{1,0:T(8,128)S(1)} %get-tuple-element.9.k_ref, bf16[1024,256]{1,0:T(8,128)(2,1)S(1)} %get-tuple-element.10.v_ref, f32[1024,256]{1,0:T(8,128)S(1)} %get-tuple-element.6.lf_ref, f32[2,128,128]{2,1,0:T(8,128)S(1)} %fusion.18.s_ref, ...), custom_call_target="tpu_custom_call" | custom-call | flops 1048576000 | bytes 3670016 | tf_op jit(solution)/shard_map/rec_out/pallas_call | solution.py:107
  218.1 1.0 copy.48
  219.1 4.4 %all-to-all-start.1 = ((bf16[4,256,256]{1,2,0:T(8,128)(2,1)}), bf16[4,256,256]{1,2,0:T(8,128)(2,1)}, u32[]{:S(2)}, u32[]{:S(2)}) async-start(bf16[4,256,256]{1,2,0:T(8,128)(2,1)} %copy.48), calls=%async_computation.1 | async-start | bytes 1048576 | tf_op jit(solution)/shard_map/all_to_all | solution.py:334
  223.5 1.6 copy-done.1
  225.1 0.9 copy-done.2
  226.0 41.5 %attend.1 = bf16[512,256]{1,0:T(8,128)(2,1)S(1)} custom-call(s32[1]{0:T(128)} %bitcast.18.refs_0_, bf16[8,96,256]{2,1,0:T(8,128)(2,1)S(1)} %maximum_bitcast_fusion.refs_1_, bf16[4096,256]{1,0:T(8,128)(2,1)S(1)} %copy-done.1, bf16[32,4096]{1,0:T(8,128)(2,1)S(1)} %copy-done.2, bf16[512,256]{1,0:T(8,128)(2,1)S(1)} %bitcast.72, bf16[512,256]{1,0:T(8,128)(2,1)S(1)} %bitcast.73), custom_call_target="tpu_custom_call" | custom-call | flops 16777216000 | bytes 2097152 | tf_op jit(solution)/shard_map/attend/pallas_call | solution.py:205
  267.6 3.6 %fusion.29 = f32[256,2048]{1,0:T(8,128)S(1)} fusion(bf16[256,1024]{0,1:T(8,128)(2,1)} %bitcast.17, bf16[1024,2048]{1,0:T(8,128)(2,1)} %param.34), kind=kOutput, calls=%fused_computation.71 | convolution fusion | flops 1073741824 | bytes 6815744 | tf_op jit(solution)/shard_map/dot_general | solution.py:336
  271.2 0.7 convolution_add_fusion
  272.0 1.3 copy-done.4
  273.3 0.1 dynamic-slice_convert_fusion
  273.4 2.7 collective-permute-start.3
  276.1 1.5 collective-permute-done.3
  277.6 2.1 add_convert_fusion
  (41 shorter events, 0.3 us)
Async XLA Ops:
  6.5 264.7 %copy-start = (bf16[512,2048]{1,0:T(8,128)(2,1)S(1)}, bf16[512,2048]{1,0:T(8,128)(2,1)}, u32[]{:S(2)}) copy-start(bf16[512,2048]{1,0:T(8,128)(2,1)} %param.35) | copy-start | bytes 6291460
  6.5 46.4 %all-gather.5.cloned.1.call-start = ((), (), s32[]{:S(2)}) async-start(), calls=%async_computation.2 | async-start | bytes 2621440 | tf_op jit(solution)/shard_map/all_gather | solution.py:270
  7.3 113.9 %all-gather.9.cloned.1.call-start = ((), (), s32[]{:S(2)}) async-start(), calls=%async_computation.4 | async-start | bytes 2506752 | tf_op jit(solution)/shard_map/all_gather | solution.py:297
  7.3 2.5 collective-permute-start.1
  9.2 1.7 copy-start.13
  9.3 1.7 copy-start.14
  11.9 1.7 copy-start.12
  11.9 2.6 copy-start.6
  11.9 2.8 copy-start.7
  11.9 2.9 %copy-start.8 = (bf16[128,1024]{1,0:T(8,128)(2,1)S(1)}, bf16[128,1024]{1,0:T(8,128)(2,1)}, u32[]{:S(2)}) copy-start(bf16[128,1024]{1,0:T(8,128)(2,1)} %param.21) | copy-start | bytes 786436
  11.9 1.5 collective-permute-start.2
  14.4 171.2 %all-gather.7.cloned.1.call-start = ((), (), s32[]{:S(2)}) async-start(), calls=%async_computation.3 | async-start | bytes 3932160 | tf_op jit(solution)/shard_map/all_gather | solution.py:266
  15.1 19.6 %copy-start.9 = (bf16[256,512]{1,0:T(8,128)(2,1)S(1)}, bf16[256,512]{1,0:T(8,128)(2,1)}, u32[]{:S(2)}) copy-start(bf16[256,512]{1,0:T(8,128)(2,1)} %param.32) | copy-start | bytes 786436
  34.8 20.1 %copy-start.11 = (f32[512]{0:T(512)S(1)}, f32[512]{0:T(512)}, u32[]{:S(2)}) copy-start(f32[512]{0:T(512)} %param.28) | copy-start | bytes 6148
  45.0 14.4 %copy-start.10 = (f32[256,16]{0,1:T(8,128)S(1)}, f32[256,16]{0,1:T(8,128)}, u32[]{:S(2)}) copy-start(f32[256,16]{0,1:T(8,128)} %get-tuple-element.28) | copy-start | bytes 49156
  52.9 77.1 %collective-permute-start = (bf16[1024,1024]{1,0:T(8,128)(2,1)}, bf16[1024,1024]{1,0:T(8,128)(2,1)}, u32[]{:S(2)}, u32[]{:S(2)}) collective-permute-start(bf16[1024,1024]{1,0:T(8,128)(2,1)} %all-gather.5.cloned.1.call-done), channel_id=1, source_target_pairs={{0,1},{1,0},{2,3},{3,2},{4,5},{5,4},{6,7},{7,6},{8,9},{9,8},{10,11... | collective-permute-start | bytes 6291464 | tf_op jit(solution)/shard_map/ppermute | solution.py:224
  192.2 1.0 copy-start.5
  194.4 0.7 copy-start.3
  219.1 48.4 %all-to-all-start.1 = ((bf16[4,256,256]{1,2,0:T(8,128)(2,1)}), bf16[4,256,256]{1,2,0:T(8,128)(2,1)}, u32[]{:S(2)}, u32[]{:S(2)}) async-start(bf16[4,256,256]{1,2,0:T(8,128)(2,1)} %copy.48), calls=%async_computation.1 | async-start | bytes 1048576 | tf_op jit(solution)/shard_map/all_to_all | solution.py:334
  223.5 1.6 copy-start.1
  225.1 0.9 copy-start.2
  272.0 1.3 copy-start.4
  273.4 4.2 %collective-permute-start.3 = (bf16[128,2048]{1,0:T(8,128)(2,1)S(1)}, bf16[128,2048]{1,0:T(8,128)(2,1)S(1)}, u32[]{:S(2)}, u32[]{:S(2)}) collective-permute-start(bf16[128,2048]{1,0:T(8,128)(2,1)S(1)} %dynamic-slice_convert_fusion), channel_id=1, source_target_pairs={{0,1},{1,0},{2,3},{3,2},{4,5},{5,4},{6,7},{7,6},{8,9},{9,8},{10,11... | collective-permute-start | bytes 1572872 | tf_op jit(solution)/shard_map/ppermute | solution.py:346
Sparse Core Ops, SparseCore 0:
  9.2 43.6 all-gather.4
  55.6 65.4 all-gather.8
  122.7 62.8 all-gather.6
